TPU v7x, 32 devices: a whole 2x2x4 slice. The times are simulated.
32 devices in a mesh: fs: 8 (over z, y), tp: 4 (over x, core).
Axes of the slice: x: 2, y: 2, z: 4, core: 2. Of those that a mesh axis runs over, the one named last changes fastest.
Arguments:
- saved_input: bfloat16 [65536, 2048], P(('fs', 'tp')), may hold values from -500 to 500
- value_cotangent: bfloat16 [65536, 1024], P(('fs', 'tp')), may hold values from -500 to 500
- hidden_input: bfloat16 [65536, 1024], P(('fs', 'tp')), may hold values from -500 to 500
- out_cotangent: bfloat16 [65536, 2048], P(('fs', 'tp')), may hold values from -500 to 500
- value_factor: bfloat16 [2048, 256], P('fs'), may hold values from -2 to 2
- out_factor: bfloat16 [1024, 256], P('fs'), may hold values from -2 to 2
- value_weight: float32 [2048, 1024], P('fs', 'tp'), may hold values from -0.125 to 0.125
- out_weight: float32 [1024, 2048], P('fs', 'tp'), may hold values from -0.1875 to 0.1875
- value_first: float32 [256, 1024], P('fs', 'tp'), may hold values from -1.2 to 1.2
- value_second: float32 [256, 1024], P('fs', 'tp'), may hold values from 0.02 to 0.5
- out_first: float32 [256, 2048], P('fs', 'tp'), may hold values from -1.2 to 1.2
- out_second: float32 [256, 2048], P('fs', 'tp'), may hold values from 0.02 to 0.5
Outputs:
- value_update: float32 [2048, 1024], P('fs', 'tp')
- out_update: float32 [1024, 2048], P('fs', 'tp')
- new_value_weight: float32 [2048, 1024], P('fs', 'tp')
- new_out_weight: float32 [1024, 2048], P('fs', 'tp')
- value_copy: bfloat16 [2048, 1024], P(None, 'tp')
- out_copy: bfloat16 [1024, 2048], P(None, 'tp')
- new_value_first: float32 [256, 1024], P('fs', 'tp')
- new_value_second: float32 [256, 1024], P('fs', 'tp')
- new_out_first: float32 [256, 2048], P('fs', 'tp')
- new_out_second: float32 [256, 2048], P('fs', 'tp')
All inputs are finite; a program needn't handle non-finite values.
Results may differ from a plain program's by a relative error of at most 0.0065.
Values may be sent and summed in bfloat16 or wider, within the bound.
A program may use at most 128 MiB of HBM per device.

v0:
```python
import jax
import jax.numpy as jnp
from jax import lax
from jax.sharding import PartitionSpec as P

D = 2048
DM = 1024
R = 256
momentum_decay = 0.9
square_decay = 0.95
adam_epsilon = 1e-08
update_scale = 0.25
learning_rate = 0.01


def moment_ratio(first, second, lowrank, clip_factor):
    scaled = clip_factor * lowrank
    new_first = momentum_decay * first + (1.0 - momentum_decay) * scaled
    new_second = square_decay * second + (1.0 - square_decay) * scaled * scaled
    ratio = new_first / (jnp.sqrt(new_second) + adam_epsilon)
    return (new_first, new_second, ratio)


def input_times_factor(inputs, factor):
    return jnp.dot(
        inputs, lax.all_gather(factor, "fs", axis=0, tiled=True), preferred_element_type=jnp.float32
    )


def split_product(basis, cotangents):
    basis_high = basis.astype(jnp.bfloat16)
    basis_rest = (basis - basis_high.astype(jnp.float32)).astype(jnp.bfloat16)
    high_part = jnp.einsum("tr,tc->rc", basis_high, cotangents, preferred_element_type=jnp.float32)
    rest_part = jnp.einsum("tr,tc->rc", basis_rest, cotangents, preferred_element_type=jnp.float32)
    return high_part + rest_part


def shards(
    saved_input,
    value_cotangent,
    hidden_input,
    out_cotangent,
    value_factor,
    out_factor,
    value_weight,
    out_weight,
    value_first,
    value_second,
    out_first,
    out_second,
):
    highest = lax.Precision.HIGHEST
    value_basis = input_times_factor(saved_input, value_factor)
    out_basis = input_times_factor(hidden_input, out_factor)
    left = value_basis
    right = out_basis
    first_part = split_product(left, value_cotangent)
    second_part = split_product(right, out_cotangent)
    lowrank = lax.psum_scatter(
        jnp.concatenate([first_part, second_part], axis=1), "fs", scatter_dimension=0, tiled=True
    )
    low_value, low_out = (
        lax.psum_scatter(lowrank[:, :DM], "tp", scatter_dimension=1, tiled=True),
        lax.psum_scatter(lowrank[:, DM:], "tp", scatter_dimension=1, tiled=True),
    )
    squares = lax.psum((jnp.sum(low_value * low_value), jnp.sum(low_out * low_out)), ("fs", "tp"))
    root_mean = jnp.sqrt((squares[0] + squares[1]) / (R * (D + DM)))
    clip_factor = 1.0 / jnp.maximum(root_mean, 1.0)
    new_value_first, new_value_second, value_ratio = moment_ratio(
        value_first, value_second, low_value, clip_factor
    )
    new_out_first, new_out_second, out_ratio = moment_ratio(
        out_first, out_second, low_out, clip_factor
    )
    left = value_factor.astype(jnp.float32)
    right = out_factor.astype(jnp.float32)
    value_sum = jnp.dot(
        left, lax.all_gather(value_ratio, "fs", axis=0, tiled=True), precision=highest
    )
    out_sum = jnp.dot(right, lax.all_gather(out_ratio, "fs", axis=0, tiled=True), precision=highest)
    value_update = update_scale * value_sum
    out_update = update_scale * out_sum
    new_value_weight = value_weight - learning_rate * value_update
    new_out_weight = out_weight - learning_rate * out_update
    value_copy, out_copy = (
        lax.all_gather(new_value_weight.astype(jnp.bfloat16), "fs", axis=0, tiled=True),
        lax.all_gather(new_out_weight.astype(jnp.bfloat16), "fs", axis=0, tiled=True),
    )
    return (
        value_update,
        out_update,
        new_value_weight,
        new_out_weight,
        value_copy,
        out_copy,
        new_value_first,
        new_value_second,
        new_out_first,
        new_out_second,
    )


def solution(mesh):
    placed = (
        P(("fs", "tp"), None),
        P(("fs", "tp"), None),
        P(("fs", "tp"), None),
        P(("fs", "tp"), None),
        P("fs", None),
        P("fs", None),
        P("fs", "tp"),
        P("fs", "tp"),
        P("fs", "tp"),
        P("fs", "tp"),
        P("fs", "tp"),
        P("fs", "tp"),
    )
    return jax.shard_map(
        shards,
        mesh=mesh,
        in_specs=placed,
        out_specs=(
            P("fs", "tp"),
            P("fs", "tp"),
            P("fs", "tp"),
            P("fs", "tp"),
            P(None, "tp"),
            P(None, "tp"),
            P("fs", "tp"),
            P("fs", "tp"),
            P("fs", "tp"),
            P("fs", "tp"),
        ),
        check_vma=False,
    )
```

profile of v0, /device:TPU:0, one launch (start us, length us, event | category | flops | bytes accessed | tf_op | source)
XLA Modules:
  0.0 351.5 jit_solution(5440025133149684813)
XLA Ops:
  8.0 33.6 %all_gather.19 = bf16[1024,256]{1,0:T(8,128)(2,1)S(1)} all-gather(bf16[128,256]{1,0:T(8,128)(2,1)} %param.17), channel_id=1, replica_groups=mesh['fs'=8,'tp'=4] {'fs'}, dimensions={0}, use_global_device_ids=true | all-gather | bytes 589824 | tf_op jit(solution)/shard_map/all_gather | solution.py:26
  41.6 3.4 fusion.13
  45.1 2.3 fusion.1
  47.4 2.4 convolution_add_fusion
  49.8 4.3 %all-gather.4.cloned.1.call-done = bf16[2048,256]{1,0:T(8,128)(2,1)} async-done(((bf16[256,256]{1,0:T(8,128)(2,1)}), bf16[2048,256]{1,0:T(8,128)(2,1)}) %all-gather.4.cloned.1.call-update) | async-done | bytes 1048592 | tf_op jit(solution)/shard_map/all_gather | solution.py:26
  54.1 6.2 %fusion.12 = f32[2048,256]{1,0:T(8,128)S(1)} fusion(bf16[2048,2048]{1,0:T(8,128)(2,1)} %param.12, bf16[2048,256]{1,0:T(8,128)(2,1)} %all-gather.4.cloned.1.call-done), kind=kOutput, calls=%fused_computation.27 | convolution fusion | flops 2147483648 | bytes 11534336 | tf_op jit(solution)/shard_map/dot_general | solution.py:25
  60.3 1.3 fusion.4
  62.9 1.9 pad_maximum_fusion
  64.9 73.3 %reduce-scatter.4.cloned.1.call-done = f32[32,3072]{1,0:T(8,128)} async-done(((f32[256,3072]{1,0:T(8,128)}), f32[32,3072]{1,0:T(8,128)}) %reduce-scatter.4.cloned.1.call-update) | async-done | bytes 393232 | tf_op jit(solution)/shard_map/reduce_scatter | solution.py:59
  138.3 1.6 slice.8
  139.9 1.7 slice.9
  141.7 18.4 %reduce-scatter.6.cloned.1.call-done = f32[32,256]{1,0:T(8,128)} async-done(((f32[32,1024]{1,0:T(8,128)}), f32[32,256]{1,0:T(8,128)}) %reduce-scatter.6.cloned.1.call-update) | async-done | bytes 32784 | tf_op jit(solution)/shard_map/reduce_scatter | solution.py:63
  160.1 1.4 multiply_reduce_fusion.1
  161.5 21.6 %reduce-scatter.8.cloned.1.call-done = f32[32,512]{1,0:T(8,128)} async-done(((f32[32,2048]{1,0:T(8,128)}), f32[32,512]{1,0:T(8,128)}) %reduce-scatter.8.cloned.1.call-update) | async-done | bytes 65552 | tf_op jit(solution)/shard_map/reduce_scatter | solution.py:64
  183.1 1.5 multiply_reduce_fusion
  186.0 39.3 %psum.16 = f32[]{:T(128)} all-reduce(f32[]{:T(128)S(6)} %add.45), channel_id=1, replica_groups=mesh['fs'=8,'tp'=4] {'fs','tp'}, use_global_device_ids=true, to_apply=%region_3.0 | all-reduce | flops 1 | bytes 8 | tf_op jit(solution)/shard_map/psum | solution.py:66
  226.0 1.5 add_divide_fusion
  227.6 31.2 %all_gather.21 = f32[256,512]{1,0:T(8,128)S(1)} all-gather(f32[32,512]{1,0:T(8,128)S(1)} %get-tuple-element.24), channel_id=1, replica_groups=mesh['fs'=8,'tp'=4] {'fs'}, dimensions={0}, use_global_device_ids=true | all-gather | bytes 589824 | tf_op jit(solution)/shard_map/all_gather | solution.py:80
  258.8 1.3 fusion.8
  261.0 31.0 %all_gather.20 = f32[256,256]{1,0:T(8,128)S(1)} all-gather(f32[32,256]{1,0:T(8,128)S(1)} %get-tuple-element.27), channel_id=1, replica_groups=mesh['fs'=8,'tp'=4] {'fs'}, dimensions={0}, use_global_device_ids=true | all-gather | bytes 294912 | tf_op jit(solution)/shard_map/all_gather | solution.py:78
  296.4 5.1 %all-gather.8.cloned.1.call-done = bf16[1024,512]{0,1:T(8,128)(2,1)} async-done(((bf16[128,512]{0,1:T(8,128)(2,1)}), bf16[1024,512]{0,1:T(8,128)(2,1)}) %all-gather.8.cloned.1.call-update) | async-done | bytes 1048592 | tf_op jit(solution)/shard_map/all_gather | solution.py:87
  301.5 2.3 copy.29
  303.8 38.6 %all-gather.6.cloned.1.call-done = bf16[2048,256]{0,1:T(8,128)(2,1)} async-done(((bf16[256,256]{0,1:T(8,128)(2,1)}), bf16[2048,256]{0,1:T(8,128)(2,1)}) %all-gather.6.cloned.1.call-update) | async-done | bytes 1048592 | tf_op jit(solution)/shard_map/all_gather | solution.py:86
  342.4 2.3 copy.28
  (45 shorter events, 7.7 us)
Async XLA Ops:
  7.2 46.9 %all-gather.4.cloned.1.call-start = ((), (), s32[]{:S(2)}) async-start(), calls=%async_computation.3 | async-start | bytes 1179648 | tf_op jit(solution)/shard_map/all_gather | solution.py:26
  7.9 130.4 %reduce-scatter.4.cloned.1.call-start = ((), (), s32[]{:S(2)}) async-start(), calls=%async_computation.4 | async-start | bytes 3538944 | tf_op jit(solution)/shard_map/reduce_scatter | solution.py:59
  8.0 37.1 %copy-start = (bf16[2048,2048]{1,0:T(8,128)(2,1)S(1)}, bf16[2048,2048]{1,0:T(8,128)(2,1)}, u32[]{:S(2)}) copy-start(bf16[2048,2048]{1,0:T(8,128)(2,1)} %param.15) | copy-start | bytes 25165828
  54.1 6.3 %copy-start.10 = (bf16[2048,1024]{1,0:T(8,128)(2,1)S(1)}, bf16[2048,1024]{1,0:T(8,128)(2,1)}, u32[]{:S(2)}) copy-start(bf16[2048,1024]{1,0:T(8,128)(2,1)} %param.13) | copy-start | bytes 12582916
  64.8 121.0 %copy-start.3 = (f32[128,512]{1,0:T(8,128)S(1)}, f32[128,512]{1,0:T(8,128)}, u32[]{:S(2)}) copy-start(f32[128,512]{1,0:T(8,128)} %param.19) | copy-start | bytes 786436
  64.8 161.2 %copy-start.6 = (f32[32,512]{1,0:T(8,128)S(1)}, f32[32,512]{1,0:T(8,128)}, u32[]{:S(2)}) copy-start(f32[32,512]{1,0:T(8,128)} %param.23) | copy-start | bytes 196612
  64.8 161.2 %copy-start.7 = (f32[32,512]{1,0:T(8,128)S(1)}, f32[32,512]{1,0:T(8,128)}, u32[]{:S(2)}) copy-start(f32[32,512]{1,0:T(8,128)} %param.22) | copy-start | bytes 196612
  64.8 194.0 %copy-start.2 = (bf16[128,256]{1,0:T(8,128)(2,1)S(1)}, bf16[128,256]{1,0:T(8,128)(2,1)}, u32[]{:S(2)}) copy-start(bf16[128,256]{1,0:T(8,128)(2,1)} %param.17) | copy-start | bytes 196612
  64.8 195.3 %copy-start.4 = (f32[256,256]{1,0:T(8,128)S(1)}, f32[256,256]{1,0:T(8,128)}, u32[]{:S(2)}) copy-start(f32[256,256]{1,0:T(8,128)} %param.18) | copy-start | bytes 786436
  64.8 195.4 %copy-start.8 = (f32[32,256]{1,0:T(8,128)S(1)}, f32[32,256]{1,0:T(8,128)}, u32[]{:S(2)}) copy-start(f32[32,256]{1,0:T(8,128)} %param.21) | copy-start | bytes 98308
  64.9 195.4 %copy-start.9 = (f32[32,256]{1,0:T(8,128)S(1)}, f32[32,256]{1,0:T(8,128)}, u32[]{:S(2)}) copy-start(f32[32,256]{1,0:T(8,128)} %param.20) | copy-start | bytes 98308
  64.9 227.1 %copy-start.1 = (bf16[256,256]{1,0:T(8,128)(2,1)S(1)}, bf16[256,256]{1,0:T(8,128)(2,1)}, u32[]{:S(2)}) copy-start(bf16[256,256]{1,0:T(8,128)(2,1)} %param.16) | copy-start | bytes 393220
  64.9 95.2 %reduce-scatter.6.cloned.1.call-start = ((), (), s32[]{:S(2)}) async-start(), calls=%async_computation.5 | async-start | bytes 163840 | tf_op jit(solution)/shard_map/reduce_scatter | solution.py:63
  139.9 43.2 %reduce-scatter.8.cloned.1.call-start = ((), (), s32[]{:S(2)}) async-start(), calls=%async_computation.6 | async-start | bytes 327680 | tf_op jit(solution)/shard_map/reduce_scatter | solution.py:64
  141.6 159.9 %all-gather.8.cloned.1.call-start = ((), (), s32[]{:S(2)}) async-start(), calls=%async_computation.8 | async-start | bytes 1179648 | tf_op jit(solution)/shard_map/all_gather | solution.py:87
  160.1 100.2 %copy-start.5 = (f32[32,256]{1,0:T(8,128)S(1)}, f32[32,256]{1,0:T(8,128)}, u32[]{:S(2)}) copy-start(f32[32,256]{1,0:T(8,128)} %reduce-scatter.6.cloned.1.call-done) | copy-start | bytes 98308
  260.1 82.4 %all-gather.6.cloned.1.call-start = ((), (), s32[]{:S(2)}) async-start(), calls=%async_computation.7 | async-start | bytes 1179648 | tf_op jit(solution)/shard_map/all_gather | solution.py:86
Sparse Core Ops, SparseCore 0:
  10.1 43.9 all-gather.3
  65.0 73.2 reduce-scatter.3
  141.3 18.7 reduce-scatter.5
  162.9 20.0 reduce-scatter.7
  260.2 41.2 all-gather.7
  304.0 38.3 all-gather.5
where the time goes:
time: 352 us
  waiting for transfers between devices  162 us (46%)
  blocking collectives  135 us (38%)
  matrix products  19.3 us (5%)
  between operations  16.3 us (5%)
  local copies, waits for them, and re-layouts  11.4 us (3%)
  other arithmetic  7.01 us (2%)
    reduce_scatter x1, waiting for transfers between devices, shards(): lax.psum_scatter(jnp.concatenate([first_part, second_part], axis=1), 'fs'...  73.3 us
    psum x1, blocking collectives, shards(): lax.psum((jnp.sum(low_value * low_value), jnp.sum(low_out * low_out)), ('...  39.3 us
    all_gather x1, waiting for transfers between devices, shards(): lax.all_gather(new_value_weight.astype(jnp.bfloat16), 'fs', axis=0, tiled...  38.6 us
    all_gather x1, blocking collectives, input_times_factor(): lax.all_gather(factor, 'fs', axis=0, tiled=True)  33.6 us
    all_gather x1, blocking collectives, shards(): lax.all_gather(out_ratio, 'fs', axis=0, tiled=True)  31.2 us
    all_gather x1, blocking collectives, shards(): lax.all_gather(value_ratio, 'fs', axis=0, tiled=True)  31 us
    reduce_scatter x1, waiting for transfers between devices, shards(): lax.psum_scatter(lowrank[:, DM:], 'tp', scatter_dimension=1, tiled=True)  21.6 us
    reduce_scatter x1, waiting for transfers between devices, shards(): lax.psum_scatter(lowrank[:, :DM], 'tp', scatter_dimension=1, tiled=True)  18.4 us
  transfers between devices with their start and end apart: 6, of which 6 were waited for; matrix products, arithmetic and copies ran while one was open for 5% of the time, Pallas kernels for 0%

commit v1 on v0

--- a/solution.py
+++ b/solution.py
@@ -11,6 +11,18 @@
 adam_epsilon = 1e-08
 update_scale = 0.25
 learning_rate = 0.01
+
+
+def doubled_up(x, axis, dim):
+    ways, here = (lax.axis_size(axis), lax.axis_index(axis))
+    grown, reach = (x, 1)
+    while reach < ways:
+        theirs = lax.ppermute(grown, axis, [(d, d ^ reach) for d in range(ways)])
+        mine_first = jnp.concatenate([grown, theirs], axis=dim)
+        theirs_first = jnp.concatenate([theirs, grown], axis=dim)
+        grown = jnp.where(here & reach == 0, mine_first, theirs_first)
+        reach = 2 * reach
+    return grown
 
 
 def moment_ratio(first, second, lowrank, clip_factor):
@@ -74,9 +86,7 @@
     )
     left = value_factor.astype(jnp.float32)
     right = out_factor.astype(jnp.float32)
-    value_sum = jnp.dot(
-        left, lax.all_gather(value_ratio, "fs", axis=0, tiled=True), precision=highest
-    )
+    value_sum = jnp.dot(left, doubled_up(value_ratio, "fs", 0), precision=highest)
     out_sum = jnp.dot(right, lax.all_gather(out_ratio, "fs", axis=0, tiled=True), precision=highest)
     value_update = update_scale * value_sum
     out_update = update_scale * out_sum

time: 352 us -> 352 us (level)
  blocking collectives: 135 us -> 104 us
  waiting for transfers between devices: 162 us -> 190 us
    all_gather x1 -> x0, blocking collectives: 31 us -> none  [shards(): lax.all_gather(value_ratio, 'fs', axis=0, tiled=True)]
    all_gather x1, waiting for transfers between devices: 5.13 us -> 19.3 us  [shards(): lax.all_gather(new_out_weight.astype(jnp.bfloat16), 'fs', axis=0, tiled=T...]
    ppermute x0 -> x3, waiting for transfers between devices: none -> 13.2 us  [doubled_up(): theirs = lax.ppermute(grown, axis, [(d, d ^ reach) for d in range(ways)])]
  transfers between devices with their start and end apart: 6 -> 9, of which waited for: 6 -> 9; matrix products, arithmetic and copies ran while one was open for 5% -> 5% of each run, Pallas kernels for 0% -> 0%
where the time goes in v1:
time: 352 us; the launch traced here: 351 us
  waiting for transfers between devices  190 us (54%)
  blocking collectives  104 us (30%)
  matrix products  19.3 us (5%)
  between operations  16.4 us (5%)
  local copies, waits for them, and re-layouts  11.4 us (3%)
  other arithmetic  7.03 us (2%)
    reduce_scatter x1, waiting for transfers between devices, shards(): lax.psum_scatter(jnp.concatenate([first_part, second_part], axis=1), 'fs'...  73.4 us
    psum x1, blocking collectives, shards(): lax.psum((jnp.sum(low_value * low_value), jnp.sum(low_out * low_out)), ('...  39.3 us
    all_gather x1, waiting for transfers between devices, shards(): lax.all_gather(new_value_weight.astype(jnp.bfloat16), 'fs', axis=0, tiled...  38.6 us
    all_gather x1, blocking collectives, input_times_factor(): lax.all_gather(factor, 'fs', axis=0, tiled=True)  33.6 us
    all_gather x1, blocking collectives, shards(): lax.all_gather(out_ratio, 'fs', axis=0, tiled=True)  31.2 us
    reduce_scatter x1, waiting for transfers between devices, shards(): lax.psum_scatter(lowrank[:, DM:], 'tp', scatter_dimension=1, tiled=True)  21.6 us
    all_gather x1, waiting for transfers between devices, shards(): lax.all_gather(new_out_weight.astype(jnp.bfloat16), 'fs', axis=0, tiled=T...  19.3 us
    reduce_scatter x1, waiting for transfers between devices, shards(): lax.psum_scatter(lowrank[:, :DM], 'tp', scatter_dimension=1, tiled=True)  18.4 us
  transfers between devices with their start and end apart: 9, of which 9 were waited for; matrix products, arithmetic and copies ran while one was open for 5% of the time, Pallas kernels for 0%

profile of v1, /device:TPU:0, one launch (start us, length us, event | category | flops | bytes accessed | tf_op | source)
XLA Modules:
  0.0 351.2 jit_solution(12720617944059998353)
XLA Ops:
  8.0 33.6 %all_gather.16 = bf16[1024,256]{1,0:T(8,128)(2,1)S(1)} all-gather(bf16[128,256]{1,0:T(8,128)(2,1)} %param.17), channel_id=1, replica_groups=mesh['fs'=8,'tp'=4] {'fs'}, dimensions={0}, use_global_device_ids=true | all-gather | bytes 589824 | tf_op jit(solution)/shard_map/all_gather | solution.py:38
  41.6 3.4 fusion.21
  45.1 2.3 fusion.1
  47.4 2.4 convolution_add_fusion
  49.8 4.3 %all-gather.4.cloned.1.call-done = bf16[2048,256]{1,0:T(8,128)(2,1)} async-done(((bf16[256,256]{1,0:T(8,128)(2,1)}), bf16[2048,256]{1,0:T(8,128)(2,1)}) %all-gather.4.cloned.1.call-update) | async-done | bytes 1048592 | tf_op jit(solution)/shard_map/all_gather | solution.py:38
  54.1 6.2 %fusion.20 = f32[2048,256]{1,0:T(8,128)S(1)} fusion(bf16[2048,2048]{1,0:T(8,128)(2,1)} %param.12, bf16[2048,256]{1,0:T(8,128)(2,1)} %all-gather.4.cloned.1.call-done), kind=kOutput, calls=%fused_computation.38 | convolution fusion | flops 2147483648 | bytes 11534336 | tf_op jit(solution)/shard_map/dot_general | solution.py:37
  62.9 1.9 pad_maximum_fusion
  64.9 73.4 %reduce-scatter.4.cloned.1.call-done = f32[32,3072]{1,0:T(8,128)} async-done(((f32[256,3072]{1,0:T(8,128)}), f32[32,3072]{1,0:T(8,128)}) %reduce-scatter.4.cloned.1.call-update) | async-done | bytes 393232 | tf_op jit(solution)/shard_map/reduce_scatter | solution.py:71
  138.3 1.6 slice.8
  139.9 1.7 slice.9
  141.7 18.4 %reduce-scatter.6.cloned.1.call-done = f32[32,256]{1,0:T(8,128)} async-done(((f32[32,1024]{1,0:T(8,128)}), f32[32,256]{1,0:T(8,128)}) %reduce-scatter.6.cloned.1.call-update) | async-done | bytes 32784 | tf_op jit(solution)/shard_map/reduce_scatter | solution.py:75
  161.5 21.6 %reduce-scatter.8.cloned.1.call-done = f32[32,512]{1,0:T(8,128)} async-done(((f32[32,2048]{1,0:T(8,128)}), f32[32,512]{1,0:T(8,128)}) %reduce-scatter.8.cloned.1.call-update) | async-done | bytes 65552 | tf_op jit(solution)/shard_map/reduce_scatter | solution.py:76
  186.0 39.3 %psum.16 = f32[]{:T(128)} all-reduce(f32[]{:T(128)S(6)} %add.45), channel_id=1, replica_groups=mesh['fs'=8,'tp'=4] {'fs','tp'}, use_global_device_ids=true, to_apply=%region_3.0 | all-reduce | flops 1 | bytes 8 | tf_op jit(solution)/shard_map/psum | solution.py:78
  226.0 1.5 add_divide_fusion
  227.6 31.2 %all_gather.17 = f32[256,512]{1,0:T(8,128)S(1)} all-gather(f32[32,512]{1,0:T(8,128)S(1)} %get-tuple-element.24), channel_id=1, replica_groups=mesh['fs'=8,'tp'=4] {'fs'}, dimensions={0}, use_global_device_ids=true | all-gather | bytes 589824 | tf_op jit(solution)/shard_map/all_gather | solution.py:90
  260.8 1.5 collective-permute-start
  262.3 2.4 collective-permute-done
  264.8 4.2 %collective-permute-done.1 = f32[64,256]{1,0:T(8,128)S(1)} collective-permute-done((f32[64,256]{1,0:T(8,128)S(1)}, f32[64,256]{1,0:T(8,128)S(1)}, u32[]{:S(2)}, u32[]{:S(2)}) %collective-permute-start.1) | collective-permute-done | bytes 65568 | tf_op jit(solution)/shard_map/ppermute | solution.py:20
  269.1 1.7 collective-permute-start.2
  270.9 6.5 %collective-permute-done.2 = f32[128,256]{1,0:T(8,128)S(1)} collective-permute-done((f32[128,256]{1,0:T(8,128)S(1)}, f32[128,256]{1,0:T(8,128)S(1)}, u32[]{:S(2)}, u32[]{:S(2)}) %collective-permute-start.2) | collective-permute-done | bytes 131104 | tf_op jit(solution)/shard_map/ppermute | solution.py:20
  281.8 19.3 %all-gather.8.cloned.1.call-done = bf16[1024,512]{0,1:T(8,128)(2,1)} async-done(((bf16[128,512]{0,1:T(8,128)(2,1)}), bf16[1024,512]{0,1:T(8,128)(2,1)}) %all-gather.8.cloned.1.call-update) | async-done | bytes 1048592 | tf_op jit(solution)/shard_map/all_gather | solution.py:97
  301.2 2.3 copy.29
  303.4 38.6 %all-gather.6.cloned.1.call-done = bf16[2048,256]{0,1:T(8,128)(2,1)} async-done(((bf16[256,256]{0,1:T(8,128)(2,1)}), bf16[2048,256]{0,1:T(8,128)(2,1)}) %all-gather.6.cloned.1.call-update) | async-done | bytes 1048592 | tf_op jit(solution)/shard_map/all_gather | solution.py:96
  342.1 2.3 copy.28
  (52 shorter events, 13.2 us)
Async XLA Ops:
  7.2 46.9 %all-gather.4.cloned.1.call-start = ((), (), s32[]{:S(2)}) async-start(), calls=%async_computation.3 | async-start | bytes 1179648 | tf_op jit(solution)/shard_map/all_gather | solution.py:38
  7.9 130.4 %reduce-scatter.4.cloned.1.call-start = ((), (), s32[]{:S(2)}) async-start(), calls=%async_computation.4 | async-start | bytes 3538944 | tf_op jit(solution)/shard_map/reduce_scatter | solution.py:71
  8.0 37.1 %copy-start = (bf16[2048,2048]{1,0:T(8,128)(2,1)S(1)}, bf16[2048,2048]{1,0:T(8,128)(2,1)}, u32[]{:S(2)}) copy-start(bf16[2048,2048]{1,0:T(8,128)(2,1)} %param.15) | copy-start | bytes 25165828
  54.1 6.3 %copy-start.10 = (bf16[2048,1024]{1,0:T(8,128)(2,1)S(1)}, bf16[2048,1024]{1,0:T(8,128)(2,1)}, u32[]{:S(2)}) copy-start(bf16[2048,1024]{1,0:T(8,128)(2,1)} %param.13) | copy-start | bytes 12582916
  64.8 121.1 %copy-start.3 = (f32[128,512]{1,0:T(8,128)S(1)}, f32[128,512]{1,0:T(8,128)}, u32[]{:S(2)}) copy-start(f32[128,512]{1,0:T(8,128)} %param.19) | copy-start | bytes 786436
  64.8 161.2 %copy-start.6 = (f32[32,512]{1,0:T(8,128)S(1)}, f32[32,512]{1,0:T(8,128)}, u32[]{:S(2)}) copy-start(f32[32,512]{1,0:T(8,128)} %param.23) | copy-start | bytes 196612
  64.8 161.2 %copy-start.7 = (f32[32,512]{1,0:T(8,128)S(1)}, f32[32,512]{1,0:T(8,128)}, u32[]{:S(2)}) copy-start(f32[32,512]{1,0:T(8,128)} %param.22) | copy-start | bytes 196612
  64.8 194.0 %copy-start.2 = (bf16[128,256]{1,0:T(8,128)(2,1)S(1)}, bf16[128,256]{1,0:T(8,128)(2,1)}, u32[]{:S(2)}) copy-start(bf16[128,256]{1,0:T(8,128)(2,1)} %param.17) | copy-start | bytes 196612
  64.8 195.3 %copy-start.8 = (f32[32,256]{1,0:T(8,128)S(1)}, f32[32,256]{1,0:T(8,128)}, u32[]{:S(2)}) copy-start(f32[32,256]{1,0:T(8,128)} %param.21) | copy-start | bytes 98308
  64.8 195.3 %copy-start.9 = (f32[32,256]{1,0:T(8,128)S(1)}, f32[32,256]{1,0:T(8,128)}, u32[]{:S(2)}) copy-start(f32[32,256]{1,0:T(8,128)} %param.20) | copy-start | bytes 98308
  64.9 205.9 %copy-start.4 = (f32[256,256]{1,0:T(8,128)S(1)}, f32[256,256]{1,0:T(8,128)}, u32[]{:S(2)}) copy-start(f32[256,256]{1,0:T(8,128)} %param.18) | copy-start | bytes 786436
  64.9 212.5 %copy-start.1 = (bf16[256,256]{1,0:T(8,128)(2,1)S(1)}, bf16[256,256]{1,0:T(8,128)(2,1)}, u32[]{:S(2)}) copy-start(bf16[256,256]{1,0:T(8,128)(2,1)} %param.16) | copy-start | bytes 393220
  64.9 95.2 %reduce-scatter.6.cloned.1.call-start = ((), (), s32[]{:S(2)}) async-start(), calls=%async_computation.5 | async-start | bytes 163840 | tf_op jit(solution)/shard_map/reduce_scatter | solution.py:75
  139.9 43.2 %reduce-scatter.8.cloned.1.call-start = ((), (), s32[]{:S(2)}) async-start(), calls=%async_computation.6 | async-start | bytes 327680 | tf_op jit(solution)/shard_map/reduce_scatter | solution.py:76
  141.6 159.5 %all-gather.8.cloned.1.call-start = ((), (), s32[]{:S(2)}) async-start(), calls=%async_computation.8 | async-start | bytes 1179648 | tf_op jit(solution)/shard_map/all_gather | solution.py:97
  160.1 100.1 %copy-start.5 = (f32[32,256]{1,0:T(8,128)S(1)}, f32[32,256]{1,0:T(8,128)}, u32[]{:S(2)}) copy-start(f32[32,256]{1,0:T(8,128)} %reduce-scatter.6.cloned.1.call-done) | copy-start | bytes 98308
  260.1 82.0 %all-gather.6.cloned.1.call-start = ((), (), s32[]{:S(2)}) async-start(), calls=%async_computation.7 | async-start | bytes 1179648 | tf_op jit(solution)/shard_map/all_gather | solution.py:96
  260.8 3.9 %collective-permute-start = (f32[32,256]{1,0:T(8,128)S(1)}, f32[32,256]{1,0:T(8,128)S(1)}, u32[]{:S(2)}, u32[]{:S(2)}) collective-permute-start(f32[32,256]{1,0:T(8,128)S(1)} %get-tuple-element.27), channel_id=1, source_target_pairs={{0,4},{4,0},{8,12},{12,8},{16,20},{20,16},{24,28},{28,24},{1,5},{5... | collective-permute-start | bytes 98312 | tf_op jit(solution)/shard_map/ppermute | solution.py:20
  264.7 4.3 %collective-permute-start.1 = (f32[64,256]{1,0:T(8,128)S(1)}, f32[64,256]{1,0:T(8,128)S(1)}, u32[]{:S(2)}, u32[]{:S(2)}) collective-permute-start(f32[64,256]{1,0:T(8,128)S(1)} %maximum_select_fusion.3), channel_id=1, source_target_pairs={{0,8},{4,12},{8,0},{12,4},{16,24},{20,28},{24,16},{28,20},{1,9},{5... | collective-permute-start | bytes 196616 | tf_op jit(solution)/shard_map/ppermute | solution.py:20
  269.1 8.3 %collective-permute-start.2 = (f32[128,256]{1,0:T(8,128)S(1)}, f32[128,256]{1,0:T(8,128)S(1)}, u32[]{:S(2)}, u32[]{:S(2)}) collective-permute-start(f32[128,256]{1,0:T(8,128)S(1)} %maximum_select_fusion.2), channel_id=1, source_target_pairs={{0,16},{4,20},{8,24},{12,28},{16,0},{20,4},{24,8},{28,12},{1,17},{... | collective-permute-start | bytes 393224 | tf_op jit(solution)/shard_map/ppermute | solution.py:20
Sparse Core Ops, SparseCore 0:
  10.1 43.9 all-gather.3
  65.0 73.2 reduce-scatter.3
  141.3 18.7 reduce-scatter.5
  163.0 20.0 reduce-scatter.7
  260.2 40.9 all-gather.7
  303.6 38.3 all-gather.5
